TPU v7x, 128 devices: a whole 4x4x4 slice. The times are simulated.
128 devices in a mesh: ep: 32 (over z, y, core), tp: 4 (over x).
Axes of the slice: x: 4, y: 4, z: 4, core: 2. Of those that a mesh axis runs over, the one named last changes fastest.
Arguments:
- query: bfloat16 [32768, 1024], P('ep', 'tp'), may hold values from -6 to 6
- keys: bfloat16 [32768, 1024], P('ep', 'tp'), may hold values from -6 to 6
- values: bfloat16 [32768, 2048], P('ep', 'tp'), may hold values from -6 to 6
- gate_pre: bfloat16 [32768, 2048], P('ep', 'tp'), may hold values from -6 to 6
- log_decay: float32 [16, 32768], P('tp', 'ep'), may hold values from -1 to 0
- out_weight: bfloat16 [2048, 4096], P(None, 'tp'), may hold values from -0.125 to 0.125
- expert_input: bfloat16 [8192, 4096], P(('ep', 'tp')), may hold values from -6 to 6
- norm_gain: float32 [4096], replicated, may hold values from 0.1 to 1.9
- routes: int32 [8192, 2], P(('ep', 'tp')), may hold values from 0 to 31, all different within a row; in each aligned block of 64 rows (0 to 63, 64 to 127, ...) at most 6 rows name the same one
- route_weights: float32 [8192, 2], P(('ep', 'tp')), may hold values from 0.1 to 1
- w_gate: bfloat16 [32, 4096, 1536], P('ep', None, 'tp'), may hold values from -0.09375 to 0.09375
- w_up: bfloat16 [32, 4096, 1536], P('ep', None, 'tp'), may hold values from -0.09375 to 0.09375
- w_down: bfloat16 [32, 1536, 4096], P('ep', 'tp'), may hold values from -0.15625 to 0.15625
Outputs:
- mixed: bfloat16 [32768, 4096], P('ep', 'tp')
- moe_out: bfloat16 [8192, 4096], P(('ep', 'tp'))
Inputs may be any that keep to these rules, and one draw needn't show every extreme that they name: `routes`: each row names 2 different experts; among the rows of one device no expert is named by more than 6 rows, a bound that some block reaches of some device.
All inputs are finite; a program needn't handle non-finite values.
Results may differ from a plain program's by a relative error of at most 0.018.
Values may be sent and summed in bfloat16 or wider, within the bound.
No kernel may reach another device: no remote copies, remote signals or barrier semaphores. Data moves between devices by JAX's collectives and lax.ppermute only.
A program may use at most 128 MiB of HBM per device.

v0:
```python
import jax
import jax.numpy as jnp
from jax import lax
from jax.sharding import Mesh
from jax.sharding import PartitionSpec as P

BLK = 128
EP = ("ep_0", "ep_1", "ep_2")
EP_TP = ("ep_0", "ep_1", "ep_2", "tp")


def filled_with(value, identity):
    return jax.tree.map(
        lambda part, zero: jnp.zeros_like(part) + jnp.asarray(zero, part.dtype), value, identity
    )


def prefix_by_axis(value, axes, combine, identity):
    before = start = filled_with(value, identity)
    subtotal = value
    for axis in reversed(axes):
        count, position = (lax.axis_size(axis), lax.axis_index(axis))
        pieces = jax.tree.map(
            lambda part, kind: lax.all_gather(part.astype(kind), axis),
            subtotal,
            (jnp.bfloat16, jnp.bfloat16),
        )
        inside, subtotal = (start, start)
        for k in range(count):
            passed = k < position
            subtotal = combine(
                subtotal, jax.tree.map(lambda part, own: part[k].astype(own.dtype), pieces, value)
            )
            inside = jax.tree.map(lambda new, old: jnp.where(passed, new, old), subtotal, inside)
        before = combine(inside, before)
    return before


def cut_along(value, dim, count):
    before, after = (value.shape[:dim], value.shape[dim + 1 :])
    return jnp.moveaxis(value.reshape(*before, count, -1, *after), dim, 0)


def laid_out(parts, dim):
    lengths = list(parts.shape[1:])
    lengths[dim] *= parts.shape[0]
    return jnp.moveaxis(parts, 0, dim).reshape(lengths)


def turned_blocks(parts, axes, sequence):
    inside = parts.shape[1:]
    result = parts.reshape(*(lax.axis_size(a) for a in axes), *inside)
    for k in sequence:
        result = lax.all_to_all(result, axes[k], k, k, tiled=True)
    return result.reshape(-1, *inside)


def exchange_by_chip(value, groups, sequence, split_dim, concat_dim):
    count = lax.axis_size(groups[0]) * lax.axis_size(groups[1])
    parts = cut_along(value, split_dim, count)
    return laid_out(turned_blocks(parts, groups, sequence), concat_dim)


def rotate(vectors, position_index):
    half_dim = vectors.shape[-1] // 2
    inverse = 1.0 / 10000.0 ** jnp.linspace(0.0, 1.0, half_dim, dtype=jnp.float32)
    angles = position_index[:, None] * inverse[None, :]
    cosine = jnp.cos(angles)[:, None, :]
    sine_part = jnp.sin(angles)[:, None, :]
    first_half = vectors[..., :half_dim]
    second_half = vectors[..., half_dim:]
    return jnp.concatenate(
        [
            first_half * cosine - second_half * sine_part,
            first_half * sine_part + second_half * cosine,
        ],
        axis=-1,
    )


def retention_block(state, inputs):
    query_blk, key_blk, value_blk, decay_blk = inputs
    width_blk = decay_blk.shape[1]
    running = jnp.cumsum(decay_blk, axis=1)
    spread = running[:, :, None] - running[:, None, :]
    causal = jnp.tril(jnp.ones((width_blk, width_blk), dtype=bool))[None]
    weights = jnp.where(causal, jnp.exp(jnp.where(causal, spread, 0.0)), 0.0)
    scores = jnp.einsum("hid,hjd->hij", query_blk, key_blk) * weights
    output = jnp.einsum("hij,hje->hie", scores, value_blk)
    output = output + jnp.einsum("hid,hde->hie", query_blk * jnp.exp(running)[:, :, None], state)
    closing = running[:, -1:]
    state_next = state * jnp.exp(closing)[:, :, None] + jnp.einsum(
        "hjd,hje->hde", key_blk * jnp.exp(closing - running)[:, :, None], value_blk
    )
    return (state_next, output)


def head_norm(vectors):
    centered = vectors - jnp.mean(vectors, axis=-1, keepdims=True)
    variance = jnp.mean(centered * centered, axis=-1, keepdims=True)
    return centered * lax.rsqrt(variance + 1e-06)


def chain_states(earlier, later):
    return (earlier[0] * later[0], earlier[1] * later[0][:, None, None] + later[1])


def mixer(query, keys, values, gate_pre, log_decay, out_weight):
    rows = query.shape[0]
    heads_here = log_decay.shape[0]
    head_dim = query.shape[1] // heads_here
    value_dim = values.shape[1] // heads_here
    offset = lax.axis_index(EP) * rows
    position_index = (offset + jnp.arange(rows, dtype=jnp.int32)).astype(jnp.float32)
    rotated_q = rotate(
        query.astype(jnp.float32).reshape(rows, heads_here, head_dim), position_index
    )
    rotated_k = rotate(
        keys.astype(jnp.float32).reshape(rows, heads_here, head_dim), position_index
    ) * head_dim ** (-0.5)
    value_rows = values.astype(jnp.float32).reshape(rows, heads_here, value_dim)
    block_count = rows // BLK

    def to_blocks(array):
        return array.reshape(block_count, BLK, heads_here, array.shape[-1]).transpose(0, 2, 1, 3)

    decay_blocks = log_decay.reshape(heads_here, block_count, BLK).transpose(1, 0, 2)
    start_state = jnp.zeros((heads_here, head_dim, value_dim), jnp.float32)
    final_state, outputs = lax.scan(
        retention_block,
        start_state,
        (to_blocks(rotated_q), to_blocks(rotated_k), to_blocks(value_rows), decay_blocks),
    )
    local_out = outputs.transpose(0, 2, 1, 3).reshape(rows, heads_here, value_dim)
    device_factor = jnp.exp(jnp.sum(log_decay, axis=1))
    incoming = prefix_by_axis(
        (device_factor, final_state),
        EP,
        chain_states,
        (jnp.ones((heads_here,), jnp.float32), jnp.zeros_like(final_state)),
    )
    cumulative = jnp.cumsum(log_decay, axis=1)
    reach = jnp.einsum("rhd,hde->rhe", rotated_q * jnp.exp(cumulative.T)[:, :, None], incoming[1])
    combined = local_out + reach
    gate_act = jax.nn.silu(gate_pre.astype(jnp.float32).reshape(rows, heads_here, value_dim))
    gated = (
        (gate_act * head_norm(combined)).reshape(rows, heads_here * value_dim).astype(jnp.bfloat16)
    )
    projected = jnp.dot(
        lax.all_gather(gated, "tp", axis=1, tiled=True),
        out_weight,
        preferred_element_type=jnp.float32,
    )
    return projected.astype(jnp.bfloat16)


def experts(expert_input, norm_gain, routes, route_weights, w_gate, w_up, w_down):
    token_count, width = expert_input.shape
    top_count = routes.shape[1]
    expert_count = lax.axis_size(EP)
    capacity = 3 * token_count * top_count // (2 * expert_count)
    rows_f = expert_input.astype(jnp.float32)
    centered = rows_f - jnp.mean(rows_f, axis=-1, keepdims=True)
    variance = jnp.mean(centered * centered, axis=-1, keepdims=True)
    normed = (centered * lax.rsqrt(variance + 1e-05) * norm_gain).astype(jnp.bfloat16)
    expert_ids = routes.reshape(token_count * top_count)
    expert_hits = (
        expert_ids[:, None] == jnp.arange(expert_count, dtype=jnp.int32)[None, :]
    ).astype(jnp.int32)
    earlier_hits = jnp.cumsum(expert_hits, axis=0) - expert_hits
    slot_index = jnp.sum(earlier_hits * expert_hits, axis=1)
    target = (expert_ids * capacity + slot_index).reshape(token_count, top_count)
    slot_ids = jnp.arange(expert_count * capacity, dtype=jnp.int32)
    placing = jnp.any(target[None, :, :] == slot_ids[:, None, None], axis=2).astype(jnp.bfloat16)
    outbound = jnp.dot(placing, normed, preferred_element_type=jnp.float32).astype(jnp.bfloat16)
    gate_w = w_gate[0]
    up_w = w_up[0]
    down_w = w_down[0]
    arrived = exchange_by_chip(outbound, (("ep_0", "ep_1"), "ep_2"), (1, 0), 0, 0)
    block_rows = lax.all_gather(arrived, "tp", axis=0, tiled=True)
    hidden = (
        jax.nn.silu(jnp.dot(block_rows, gate_w, preferred_element_type=jnp.float32))
        * jnp.dot(block_rows, up_w, preferred_element_type=jnp.float32)
    ).astype(jnp.bfloat16)
    summed = lax.psum_scatter(
        jnp.dot(hidden, down_w, preferred_element_type=jnp.float32).astype(jnp.bfloat16),
        "tp",
        scatter_dimension=0,
        tiled=True,
    )
    returned = lax.all_to_all(summed, EP, split_axis=0, concat_axis=0, tiled=True)
    total = jnp.zeros((token_count, width), jnp.float32)
    for route_index in range(top_count):
        picking = (target[:, route_index][:, None] == slot_ids[None, :]).astype(jnp.bfloat16)
        picked = jnp.dot(picking, returned, preferred_element_type=jnp.float32)
        total = total + route_weights[:, route_index : route_index + 1] * picked
    return total.astype(jnp.bfloat16)


def per_device(
    query,
    keys,
    values,
    gate_pre,
    log_decay,
    out_weight,
    expert_input,
    norm_gain,
    routes,
    route_weights,
    w_gate,
    w_up,
    w_down,
):
    mixed = mixer(query, keys, values, gate_pre, log_decay, out_weight)
    moe_out = experts(expert_input, norm_gain, routes, route_weights, w_gate, w_up, w_down)
    return (mixed, moe_out)


def solution(mesh):
    torus = Mesh(mesh.devices.reshape(4, 4, 2, mesh.shape["tp"]), ("ep_0", "ep_1", "ep_2", "tp"))
    return jax.shard_map(
        per_device,
        mesh=torus,
        in_specs=(
            P(EP, "tp"),
            P(EP, "tp"),
            P(EP, "tp"),
            P(EP, "tp"),
            P("tp", EP),
            P(None, "tp"),
            P(EP_TP, None),
            P(),
            P(EP_TP, None),
            P(EP_TP, None),
            P(EP, None, "tp"),
            P(EP, None, "tp"),
            P(EP, "tp", None),
        ),
        out_specs=(P(EP, "tp"), P(EP_TP, None)),
        check_vma=False,
    )
```

profile of v0, /device:TPU:1, one launch (start us, length us, event | category | flops | bytes accessed | tf_op | source)
XLA Modules:
  0.0 299.7 jit_solution(16685143774155479839)
XLA Ops:
  9.7 1.2 convert_reduce_fusion
  11.0 1.3 fusion.41
  12.3 2.9 convolution_convert_fusion.1
  15.2 3.5 %reshape_reshape.11 = bf16[16,2,6,4096]{3,2,1,0:T(8,128)(2,1)} reshape(bf16[192,4096]{1,0:T(8,128)(2,1)} %convolution_convert_fusion.1) | data formatting | bytes 3145728 | tf_op jit(solution)/shard_map/reshape;reshape | solution.py:52
  18.7 2.5 copy.79
  21.2 6.0 %all_to_all.22 = bf16[16,2,6,4096]{3,0,2,1:T(8,128)(2,1)S(1)} all-to-all(bf16[16,2,6,4096]{3,0,2,1:T(8,128)(2,1)S(1)} %copy.79), channel_id=1, replica_groups=mesh['ep_0'=4,'ep_1'=4,'ep_2'=2,'tp'=4] {'ep_2'}, dimensions={1} | all-to-all | bytes 3145728 | tf_op jit(solution)/shard_map/all_to_all | solution.py:54
  27.2 1.6 copy.80
  28.8 29.6 %all_to_all.23 = bf16[16,2,6,4096]{3,1,2,0:T(2,128)(2,1)S(1)} all-to-all(bf16[16,2,6,4096]{3,1,2,0:T(2,128)(2,1)S(1)} %copy.80), channel_id=1, replica_groups=mesh['ep_0'=4,'ep_1'=4,'ep_2'=2,'tp'=4] {'ep_0','ep_1'}, dimensions={0} | all-to-all | bytes 3145728 | tf_op jit(solution)/shard_map/all_to_all | solution.py:54
  58.4 2.3 copy.81
  60.8 3.7 %reshape_reshape.12 = bf16[192,4096]{1,0:T(8,128)(2,1)} reshape(bf16[16,2,6,4096]{3,2,1,0:T(8,128)(2,1)} %copy.81) | data formatting | bytes 3145728 | tf_op jit(solution)/shard_map/reshape;reshape | solution.py:47
  66.2 3.9 %all-reduce = bf16[8]{0:T(256)(128)(2,1)S(1)} all-reduce(bf16[8]{0:T(256)(128)(2,1)S(1)} %dynamic-update-slice), channel_id=2, replica_groups=mesh['ep_0'=4,'ep_1'=4,'ep_2'=2,'tp'=4] {'ep_2'}, use_global_device_ids=true, to_apply=%add | all-reduce | flops 8 | bytes 32
  70.2 5.5 %all-gather.2 = bf16[4,1,4]{2,1,0:T(2,128)(2,1)S(1)} all-gather(bf16[1,1,4]{2,1,0:T(2,128)(2,1)S(1)} %convert_bitcast_fusion.6), channel_id=1, replica_groups=mesh['ep_0'=4,'ep_1'=4,'ep_2'=2,'tp'=4] {'ep_1'}, dimensions={0}, use_global_device_ids=true | all-gather | bytes 40 | tf_op jit(solution)/shard_map/all_gather | solution.py:24
  75.7 6.7 %all-gather.3 = bf16[4,1,4]{2,1,0:T(2,128)(2,1)S(1)} all-gather(bf16[1,1,4]{2,1,0:T(2,128)(2,1)S(1)} %fusion.132), channel_id=1, replica_groups=mesh['ep_0'=4,'ep_1'=4,'ep_2'=2,'tp'=4] {'ep_0'}, dimensions={0}, use_global_device_ids=true | all-gather | bytes 40 | tf_op jit(solution)/shard_map/all_gather | solution.py:24
  82.3 2.1 copy.69
  84.4 2.2 convert.24
  86.6 2.1 copy.71
  88.6 2.1 convert.25
  91.4 1.9 multiply_subtract_fusion
  93.4 1.2 copy.88
  96.5 2.2 reshape.401
  98.6 2.6 copy.92
  102.3 26.4 %all-gather.9.cloned.1.call-done = bf16[768,4096]{1,0:T(8,128)(2,1)} async-done(((bf16[192,4096]{1,0:T(8,128)(2,1)}), bf16[768,4096]{1,0:T(8,128)(2,1)}) %all-gather.9.cloned.1.call-update) | async-done | bytes 6291472 | tf_op jit(solution)/shard_map/all_gather | solution.py:180
  128.7 6.6 %fusion.31 = f32[768,384]{1,0:T(8,128)S(1)} fusion(bf16[768,4096]{1,0:T(8,128)(2,1)} %all-gather.9.cloned.1.call-done, bf16[1,4096,384]{2,1,0:T(8,128)(2,1)} %param.27), kind=kOutput, calls=%fused_computation.45 | convolution fusion | flops 2415919104 | bytes 10616832 | tf_op jit(solution)/shard_map/dot_general | solution.py:182
  135.3 3.5 %fusion.36 = bf16[768,384]{1,0:T(8,128)(2,1)S(1)} fusion(bf16[768,4096]{1,0:T(8,128)(2,1)S(1)} %copy-done.12, bf16[1,4096,384]{2,1,0:T(8,128)(2,1)S(1)} %copy-done.13, f32[768,384]{1,0:T(8,128)S(1)} %fusion.31), kind=kOutput, calls=%fused_computation.53 | convolution fusion | flops 2417688576 | bytes 11206656 | tf_op jit(solution)/shard_map/dot_general | solution.py:183
  138.8 5.4 %convolution_convert_fusion = bf16[768,4096]{1,0:T(8,128)(2,1)} fusion(bf16[768,384]{1,0:T(8,128)(2,1)S(1)} %fusion.36, bf16[1,384,4096]{2,1,0:T(8,128)(2,1)S(1)} %copy-done), kind=kOutput, calls=%fused_computation.36 | convolution fusion | flops 2419064832 | bytes 10027008 | tf_op jit(solution)/shard_map/dot_general | solution.py:186
  144.3 45.7 %while.13 = (s32[]{:T(128)}, f32[4,64,128]{2,1,0:T(8,128)S(1)}, f32[8,4,128,128]{3,2,1,0:T(8,128)}, f32[8,4,128]{2,1,0:T(4,128)S(1)}, f32[8,4,128,64]{2,0,3,1:T(...) while((s32[]{:T(128)}, f32[4,64,128]{2,1,0:T(8,128)S(1)}, ...), condition=%wide.region_2.4_spmd.clone, body=%wide.region_0.3_spmd.clone.sunk | while | flops 42614784 | bytes 2547404 | solution.py:129
  144.3 1.7 constant_dynamic-slice_fusion.3
  146.4 1.3 fusion.167
  148.9 1.1 convolution_add_fusion.3
  150.0 1.7 constant_dynamic-slice_fusion.3
  152.1 1.3 fusion.167
  154.5 1.1 convolution_add_fusion.3
  155.7 1.8 constant_dynamic-slice_fusion.3
  157.8 1.3 fusion.167
  161.4 1.8 constant_dynamic-slice_fusion.3
  163.5 1.3 fusion.167
  166.0 1.1 convolution_add_fusion.3
  167.1 1.7 constant_dynamic-slice_fusion.3
  169.2 1.3 fusion.167
  172.8 1.7 constant_dynamic-slice_fusion.3
  174.9 1.3 fusion.167
  178.5 1.8 constant_dynamic-slice_fusion.3
  180.7 1.3 fusion.167
  183.2 1.1 convolution_add_fusion.3
  184.3 1.7 constant_dynamic-slice_fusion.3
  186.4 1.3 fusion.167
  188.9 1.1 convolution_add_fusion.3
  190.0 2.0 copy.75
  192.1 1.5 reshape.318
  193.6 1.1 reduce-window.6
  195.2 2.7 copy.68
  197.9 2.2 all-gather.1
  200.3 10.5 %all_gather.37 = bf16[4,4,64,128]{3,2,1,0:T(8,128)(2,1)S(1)} all-gather(bf16[1,4,64,128]{3,2,1,0:T(8,128)(2,1)S(1)} %fusion.78), channel_id=1, replica_groups=mesh['ep_0'=4,'ep_1'=4,'ep_2'=2,'tp'=4] {'ep_1'}, dimensions={0}, use_global_device_ids=true | all-gather | bytes 327680 | tf_op jit(solution)/shard_map/all_gather | solution.py:24
  211.0 9.8 %all_gather.38 = bf16[4,4,64,128]{3,2,1,0:T(8,128)(2,1)S(1)} all-gather(bf16[1,4,64,128]{3,2,1,0:T(8,128)(2,1)S(1)} %fusion.72), channel_id=1, replica_groups=mesh['ep_0'=4,'ep_1'=4,'ep_2'=2,'tp'=4] {'ep_0'}, dimensions={0}, use_global_device_ids=true | all-gather | bytes 327680 | tf_op jit(solution)/shard_map/all_gather | solution.py:24
  220.9 2.3 fusion.138
  223.5 1.3 copy-done.3
  224.8 1.6 multiply_convert_fusion
  226.4 3.5 %all_to_all.16 = bf16[32,6,4096]{2,1,0:T(8,128)(2,1)} reshape(bf16[192,4096]{1,0:T(8,128)(2,1)} %reduce-scatter.2.cloned.1.call-done) | data formatting | bytes 3145728 | tf_op jit(solution)/shard_map/all_to_all | solution.py:191
  229.9 11.2 %all-to-all-start.2 = ((bf16[32,6,4096]{2,1,0:T(8,128)(2,1)}), bf16[32,6,4096]{2,1,0:T(8,128)(2,1)S(1)}, u32[]{:S(2)}, u32[]{:S(2)}) async-start(bf16[32,6,4096]{2,1,0:T(8,128)(2,1)} %all_to_all.16), calls=%async_computation.3 | async-start | bytes 4194304 | tf_op jit(solution)/shard_map/all_to_all | solution.py:191
  241.2 37.9 %all-gather.7.cloned.1.call-done = bf16[1024,2048]{0,1:T(8,128)(2,1)} async-done(((bf16[1024,512]{0,1:T(8,128)(2,1)}), bf16[1024,2048]{0,1:T(8,128)(2,1)}) %all-gather.7.cloned.1.call-update) | async-done | bytes 4194320 | tf_op jit(solution)/shard_map/all_gather | solution.py:150
  279.1 9.4 %convolution_convert_fusion.2 = bf16[1024,1024]{1,0:T(8,128)(2,1)} fusion(bf16[1024,2048]{0,1:T(8,128)(2,1)} %all-gather.7.cloned.1.call-done, bf16[2048,1024]{1,0:T(8,128)(2,1)} %param.22), kind=kOutput, calls=%fused_computation.51 | convolution fusion | flops 4296015872 | bytes 10485760 | tf_op jit(solution)/shard_map/dot_general | solution.py:149
  288.4 1.4 all_to_all.18
  289.9 2.0 convolution_multiply_fusion.2
  291.9 1.3 fusion.27
  (134 shorter events, 24.2 us)
Async XLA Ops:
  7.2 131.6 %copy-start = (bf16[1,384,4096]{2,1,0:T(8,128)(2,1)S(1)}, bf16[1,384,4096]{2,1,0:T(8,128)(2,1)}, u32[]{:S(2)}) copy-start(bf16[1,384,4096]{2,1,0:T(8,128)(2,1)} %param.29) | copy-start | bytes 9437188
  7.2 121.5 %all-gather.9.cloned.1.call-start = ((), (), s32[]{:S(2)}) async-start(), calls=%async_computation.5 | async-start | bytes 7864320 | tf_op jit(solution)/shard_map/all_gather | solution.py:180
  60.8 3.8 %copy-start.14 = (u32[128]{0:T(128)S(1)}, u32[128]{0:T(128)}, u32[]{:S(2)}) copy-start(u32[128]{0:T(128)} %constant.100) | copy-start | bytes 1540
  60.8 5.1 %copy-start.10 = (f32[4,1024]{1,0:T(4,128)S(1)}, f32[4,1024]{1,0:T(4,128)}, u32[]{:S(2)}) copy-start(f32[4,1024]{1,0:T(4,128)} %param.21) | copy-start | bytes 49156
  64.5 161.9 %reduce-scatter.2.cloned.1.call-start = ((), (), s32[]{:S(2)}) async-start(), calls=%async_computation.6 | async-start | bytes 7864320 | tf_op jit(solution)/shard_map/reduce_scatter | solution.py:185
  93.3 1.4 copy-start.4
  93.3 1.4 copy-start.6
  98.6 2.6 copy-start.8
  98.6 2.6 copy-start.9
  128.7 6.6 %copy-start.12 = (bf16[768,4096]{1,0:T(8,128)(2,1)S(1)}, bf16[768,4096]{1,0:T(8,128)(2,1)}, u32[]{:S(2)}) copy-start(bf16[768,4096]{1,0:T(8,128)(2,1)} %all-gather.9.cloned.1.call-done) | copy-start | bytes 18874372
  128.7 6.6 %copy-start.13 = (bf16[1,4096,384]{2,1,0:T(8,128)(2,1)S(1)}, bf16[1,4096,384]{2,1,0:T(8,128)(2,1)}, u32[]{:S(2)}) copy-start(bf16[1,4096,384]{2,1,0:T(8,128)(2,1)} %param.28) | copy-start | bytes 9437188
  144.2 134.8 %all-gather.7.cloned.1.call-start = ((), (), s32[]{:S(2)}) async-start(), calls=%async_computation.4 | async-start | bytes 5242880 | tf_op jit(solution)/shard_map/all_gather | solution.py:150
  195.2 25.7 %copy-start.5 = (f32[1024,4,32]{0,2,1:T(8,128)S(1)}, f32[1024,4,32]{0,2,1:T(8,128)}, u32[]{:S(2)}) copy-start(f32[1024,4,32]{0,2,1:T(8,128)} %copy-done.4) | copy-start | bytes 1572868
  195.2 25.7 %copy-start.7 = (f32[1024,4,32]{0,2,1:T(8,128)S(1)}, f32[1024,4,32]{0,2,1:T(8,128)}, u32[]{:S(2)}) copy-start(f32[1024,4,32]{0,2,1:T(8,128)} %copy-done.6) | copy-start | bytes 1572868
  223.2 1.6 copy-start.3
  229.9 11.2 %copy-start.11 = (f32[64,2]{0,1:T(2,128)S(1)}, f32[64,2]{0,1:T(2,128)}, u32[]{:S(2)}) copy-start(f32[64,2]{0,1:T(2,128)} %param.26) | copy-start | bytes 1540
  229.9 58.5 %all-to-all-start.2 = ((bf16[32,6,4096]{2,1,0:T(8,128)(2,1)}), bf16[32,6,4096]{2,1,0:T(8,128)(2,1)S(1)}, u32[]{:S(2)}, u32[]{:S(2)}) async-start(bf16[32,6,4096]{2,1,0:T(8,128)(2,1)} %all_to_all.16), calls=%async_computation.3 | async-start | bytes 4194304 | tf_op jit(solution)/shard_map/all_to_all | solution.py:191
  289.9 2.0 copy-start.2
  289.9 3.3 %copy-start.1 = (bf16[1,384,4096]{2,1,0:T(8,128)(2,1)S(1)}, bf16[1,384,4096]{2,1,0:T(8,128)(2,1)}, u32[]{:S(2)}) copy-start(bf16[1,384,4096]{2,1,0:T(8,128)(2,1)} %param.29) | copy-start | bytes 9437188
Sparse Core Ops, SparseCore 0:
  64.6 63.9 all-gather.8
  144.3 64.7 reduce-scatter.1
  226.5 52.4 all-gather.6
where the time goes:
time: 301 us; the launch traced here: 300 us
  blocking collectives  74.3 us (25%)
  waiting for transfers between devices  64.3 us (21%)
  matrix products  59.7 us (20%)
  local copies, waits for them, and re-layouts  56.1 us (19%)
  other arithmetic  18.8 us (6%)
  between operations  14.8 us (5%)
  starting transfers between devices  11.3 us (4%)
    all_gather x1, waiting for transfers between devices, mixer(): lax.all_gather(gated, 'tp', axis=1, tiled=True)  37.9 us
    all_to_all x2, blocking collectives, turned_blocks(): result = lax.all_to_all(result, axes[k], k, k, tiled=True)  35.6 us
    all_gather x5, blocking collectives, prefix_by_axis(): lax.all_gather(part.astype(kind), axis)  34.8 us
    all_gather x1, waiting for transfers between devices, experts(): block_rows = lax.all_gather(arrived, 'tp', axis=0, tiled=True)  26.4 us
    dynamic_slice x8, local copies, waits for them, and re-layouts, mixer(): lax.scan(retention_block, start_state, (to_blocks(rotated_q), to_blocks(r...  14.1 us
    all_to_all x1, starting transfers between devices, experts(): lax.all_to_all(summed, EP, split_axis=0, concat_axis=0, tiled=True)  11.2 us
    unnamed x40, local copies, waits for them, and re-layouts  10.2 us
    dot_general x8, matrix products, retention_block(): output = jnp.einsum('hij,hje->hie', scores, value_blk)  10.2 us
  transfers between devices with their start and end apart: 4, of which 2 were waited for; matrix products, arithmetic and copies ran while one was open for 29% of the time, Pallas kernels for 0%

commit v1 on v0

--- a/solution.py
+++ b/solution.py
@@ -177,7 +177,9 @@
     up_w = w_up[0]
     down_w = w_down[0]
     arrived = exchange_by_chip(outbound, (("ep_0", "ep_1"), "ep_2"), (1, 0), 0, 0)
-    block_rows = lax.all_gather(arrived, "tp", axis=0, tiled=True)
+    block_rows = jnp.concatenate(
+        lax.all_to_all(jnp.stack([arrived] * lax.axis_size("tp")), "tp", 0, 0), axis=0
+    )
     hidden = (
         jax.nn.silu(jnp.dot(block_rows, gate_w, preferred_element_type=jnp.float32))
         * jnp.dot(block_rows, up_w, preferred_element_type=jnp.float32)

time: 301 us -> 318 us (1.056)
  local copies, waits for them, and re-layouts: 56.1 us -> 60.9 us
  starting transfers between devices: 11.3 us -> 15.5 us
    all_to_all x0 -> x1, waiting for transfers between devices: none -> 30.8 us  [experts(): lax.all_to_all(jnp.stack([arrived] * lax.axis_size('tp')), 'tp', 0, 0)]
    all_gather x1 -> x0, waiting for transfers between devices: 26.4 us -> none  [experts(): block_rows = lax.all_gather(arrived, 'tp', axis=0, tiled=True)]
    all_to_all x0 -> x1, starting transfers between devices: none -> 5.36 us  [experts(): lax.all_to_all(jnp.stack([arrived] * lax.axis_size('tp')), 'tp', 0, 0)]
    another operation x1 -> x2, local copies, waits for them, and re-layouts: 3.71 us -> 8.51 us  [experts(): jnp.stack([arrived] * lax.axis_size('tp'))]
    unnamed x40 -> x38, local copies, waits for them, and re-layouts: 10.2 us -> 10.2 us
  transfers between devices with their start and end apart: 4 -> 4, of which waited for: 2 -> 2; matrix products, arithmetic and copies ran while one was open for 29% -> 28% of each run, Pallas kernels for 0% -> 0%
where the time goes in v1:
time: 318 us; the launch traced here: 316 us
  blocking collectives  76.3 us (24%)
  waiting for transfers between devices  67.1 us (21%)
  matrix products  62.4 us (20%)
  local copies, waits for them, and re-layouts  60.9 us (19%)
  other arithmetic  18.7 us (6%)
  starting transfers between devices  15.5 us (5%)
  between operations  15.1 us (5%)
    all_gather x5, blocking collectives, prefix_by_axis(): lax.all_gather(part.astype(kind), axis)  36.8 us
    all_gather x1, waiting for transfers between devices, mixer(): lax.all_gather(gated, 'tp', axis=1, tiled=True)  36.2 us
    all_to_all x2, blocking collectives, turned_blocks(): result = lax.all_to_all(result, axes[k], k, k, tiled=True)  35.6 us
    all_to_all x1, waiting for transfers between devices, experts(): lax.all_to_all(jnp.stack([arrived] * lax.axis_size('tp')), 'tp', 0, 0)  30.8 us
    dynamic_slice x8, local copies, waits for them, and re-layouts, mixer(): lax.scan(retention_block, start_state, (to_blocks(rotated_q), to_blocks(r...  14.2 us
    unnamed x38, local copies, waits for them, and re-layouts  10.2 us
    dot_general x8, matrix products, retention_block(): output = jnp.einsum('hij,hje->hie', scores, value_blk)  10.2 us
    all_to_all x1, starting transfers between devices, experts(): lax.all_to_all(summed, EP, split_axis=0, concat_axis=0, tiled=True)  10.1 us
  transfers between devices with their start and end apart: 4, of which 2 were waited for; matrix products, arithmetic and copies ran while one was open for 28% of the time, Pallas kernels for 0%

profile of v1, /device:TPU:1, one launch (start us, length us, event | category | flops | bytes accessed | tf_op | source)
XLA Modules:
  0.0 316.4 jit_solution(6342259772320767318)
XLA Ops:
  9.7 1.2 convert_reduce_fusion
  10.9 1.3 fusion.41
  12.3 2.9 convolution_convert_fusion.1
  15.2 3.5 %reshape_reshape.8 = bf16[16,2,6,4096]{3,2,1,0:T(8,128)(2,1)} reshape(bf16[192,4096]{1,0:T(8,128)(2,1)} %convolution_convert_fusion.1) | data formatting | bytes 3145728 | tf_op jit(solution)/shard_map/reshape;reshape | solution.py:52
  18.6 2.5 copy.79
  21.1 6.0 %all_to_all.27 = bf16[16,2,6,4096]{3,0,2,1:T(8,128)(2,1)S(1)} all-to-all(bf16[16,2,6,4096]{3,0,2,1:T(8,128)(2,1)S(1)} %copy.79), channel_id=1, replica_groups=mesh['ep_0'=4,'ep_1'=4,'ep_2'=2,'tp'=4] {'ep_2'}, dimensions={1} | all-to-all | bytes 3145728 | tf_op jit(solution)/shard_map/all_to_all | solution.py:54
  27.1 1.6 copy.80
  28.7 29.6 %all_to_all.28 = bf16[16,2,6,4096]{3,1,2,0:T(2,128)(2,1)S(1)} all-to-all(bf16[16,2,6,4096]{3,1,2,0:T(2,128)(2,1)S(1)} %copy.80), channel_id=1, replica_groups=mesh['ep_0'=4,'ep_1'=4,'ep_2'=2,'tp'=4] {'ep_0','ep_1'}, dimensions={0} | all-to-all | bytes 3145728 | tf_op jit(solution)/shard_map/all_to_all | solution.py:54
  58.4 2.3 copy.81
  60.7 3.7 %stack_reshape_reshape.2 = bf16[192,4096]{1,0:T(8,128)(2,1)} reshape(bf16[16,2,6,4096]{3,2,1,0:T(8,128)(2,1)} %copy.81) | data formatting | bytes 3145728 | tf_op jit(solution)/shard_map/stack;reshape;reshape | solution.py:181
  64.4 4.9 %stack.3 = bf16[4,192,4096]{2,1,0:T(8,128)(2,1)} broadcast(bf16[192,4096]{1,0:T(8,128)(2,1)} %stack_reshape_reshape.2), dimensions={1,2} | broadcast | bytes 7864320 | tf_op jit(solution)/shard_map/stack | solution.py:181
  69.2 5.4 %all-to-all-start.2 = ((bf16[4,192,4096]{2,1,0:T(8,128)(2,1)}), bf16[4,192,4096]{2,1,0:T(8,128)(2,1)}, u32[]{:S(2)}, u32[]{:S(2)}) async-start(bf16[4,192,4096]{2,1,0:T(8,128)(2,1)} %stack.3), calls=%async_computation.2 | async-start | bytes 12582912 | tf_op jit(solution)/shard_map/all_to_all | solution.py:181
  76.3 3.9 %all-reduce = bf16[8]{0:T(256)(128)(2,1)S(1)} all-reduce(bf16[8]{0:T(256)(128)(2,1)S(1)} %dynamic-update-slice), channel_id=2, replica_groups=mesh['ep_0'=4,'ep_1'=4,'ep_2'=2,'tp'=4] {'ep_2'}, use_global_device_ids=true, to_apply=%add | all-reduce | flops 8 | bytes 32
  80.2 6.3 %all-gather.2 = bf16[4,1,4]{2,1,0:T(2,128)(2,1)S(1)} all-gather(bf16[1,1,4]{2,1,0:T(2,128)(2,1)S(1)} %convert_bitcast_fusion.6), channel_id=1, replica_groups=mesh['ep_0'=4,'ep_1'=4,'ep_2'=2,'tp'=4] {'ep_1'}, dimensions={0}, use_global_device_ids=true | all-gather | bytes 40 | tf_op jit(solution)/shard_map/all_gather | solution.py:24
  86.6 7.1 %all-gather.3 = bf16[4,1,4]{2,1,0:T(2,128)(2,1)S(1)} all-gather(bf16[1,1,4]{2,1,0:T(2,128)(2,1)S(1)} %fusion.132), channel_id=1, replica_groups=mesh['ep_0'=4,'ep_1'=4,'ep_2'=2,'tp'=4] {'ep_0'}, dimensions={0}, use_global_device_ids=true | all-gather | bytes 40 | tf_op jit(solution)/shard_map/all_gather | solution.py:24
  93.6 2.0 copy.69
  95.7 2.1 convert.24
  97.8 2.0 copy.71
  99.8 2.2 convert.25
  102.7 1.8 multiply_subtract_fusion
  104.7 1.3 copy.88
  107.7 2.1 reshape.407
  109.8 2.5 copy.92
  113.4 30.8 %all-to-all-done.2 = bf16[4,192,4096]{2,1,0:T(8,128)(2,1)} async-done(((bf16[4,192,4096]{2,1,0:T(8,128)(2,1)}), bf16[4,192,4096]{2,1,0:T(8,128)(2,1)}, u32[]{:S(2)}, u32[]{:S(2)}) %all-to-all-start.2) | async-done | bytes 6291488 | tf_op jit(solution)/shard_map/all_to_all | solution.py:181
  144.3 6.6 %fusion.31 = f32[768,384]{1,0:T(8,128)S(1)} fusion(bf16[768,4096]{1,0:T(8,128)(2,1)} %bitcast.41, bf16[1,4096,384]{2,1,0:T(8,128)(2,1)} %param.27), kind=kOutput, calls=%fused_computation.45 | convolution fusion | flops 2415919104 | bytes 10616832 | tf_op jit(solution)/shard_map/dot_general | solution.py:184
  150.9 6.3 %fusion.36 = bf16[768,384]{1,0:T(8,128)(2,1)S(1)} fusion(bf16[768,4096]{1,0:T(8,128)(2,1)} %bitcast.41, bf16[1,4096,384]{2,1,0:T(8,128)(2,1)S(1)} %copy-done.12, f32[768,384]{1,0:T(8,128)S(1)} %fusion.31), kind=kOutput, calls=%fused_computation.53 | convolution fusion | flops 2417688576 | bytes 11206656 | tf_op jit(solution)/shard_map/dot_general | solution.py:185
  157.1 5.3 %convolution_convert_fusion = bf16[768,4096]{1,0:T(8,128)(2,1)} fusion(bf16[768,384]{1,0:T(8,128)(2,1)S(1)} %fusion.36, bf16[1,384,4096]{2,1,0:T(8,128)(2,1)S(1)} %copy-done), kind=kOutput, calls=%fused_computation.36 | convolution fusion | flops 2419064832 | bytes 10027008 | tf_op jit(solution)/shard_map/dot_general | solution.py:188
  162.5 45.8 %while.13 = (s32[]{:T(128)}, f32[4,64,128]{2,1,0:T(8,128)S(1)}, f32[8,4,128,128]{3,2,1,0:T(8,128)}, f32[8,4,128]{2,1,0:T(4,128)S(1)}, f32[8,4,128,64]{2,0,3,1:T(...) while((s32[]{:T(128)}, f32[4,64,128]{2,1,0:T(8,128)S(1)}, ...), condition=%wide.region_2.4_spmd.clone, body=%wide.region_0.3_spmd.clone.sunk | while | flops 42614784 | bytes 2547404 | solution.py:129
  162.5 1.7 constant_dynamic-slice_fusion.3
  164.6 1.3 fusion.167
  168.2 1.9 constant_dynamic-slice_fusion.3
  170.5 1.3 fusion.167
  173.0 1.1 convolution_add_fusion.3
  174.1 1.7 constant_dynamic-slice_fusion.3
  176.2 1.3 fusion.167
  179.8 1.7 constant_dynamic-slice_fusion.3
  181.9 1.3 fusion.167
  185.5 1.8 constant_dynamic-slice_fusion.3
  187.6 1.3 fusion.167
  190.1 1.1 convolution_add_fusion.3
  191.2 1.7 constant_dynamic-slice_fusion.3
  193.3 1.3 fusion.167
  196.9 1.7 constant_dynamic-slice_fusion.3
  199.0 1.3 fusion.167
  202.6 1.8 constant_dynamic-slice_fusion.3
  204.8 1.3 fusion.167
  207.3 1.1 convolution_add_fusion.3
  208.4 2.0 copy.75
  210.4 1.5 reshape.323
  212.0 1.1 reduce-window.6
  213.6 2.7 copy.68
  216.2 4.4 %all-gather.1 = bf16[8,64,128]{2,1,0:T(8,128)(2,1)S(1)} all-gather(bf16[4,64,128]{2,1,0:T(8,128)(2,1)S(1)} %convert_element_type.310), channel_id=3, replica_groups=mesh['ep_0'=4,'ep_1'=4,'ep_2'=2,'tp'=4] {'ep_2'}, dimensions={0}, use_global_device_ids=true | all-gather | bytes 196608 | tf_op jit(solution)/shard_map/all_gather | solution.py:24
  220.8 9.4 %all_gather.34 = bf16[4,4,64,128]{3,2,1,0:T(8,128)(2,1)S(1)} all-gather(bf16[1,4,64,128]{3,2,1,0:T(8,128)(2,1)S(1)} %fusion.78), channel_id=1, replica_groups=mesh['ep_0'=4,'ep_1'=4,'ep_2'=2,'tp'=4] {'ep_1'}, dimensions={0}, use_global_device_ids=true | all-gather | bytes 327680 | tf_op jit(solution)/shard_map/all_gather | solution.py:24
  230.3 9.7 %all_gather.35 = bf16[4,4,64,128]{3,2,1,0:T(8,128)(2,1)S(1)} all-gather(bf16[1,4,64,128]{3,2,1,0:T(8,128)(2,1)S(1)} %fusion.72), channel_id=1, replica_groups=mesh['ep_0'=4,'ep_1'=4,'ep_2'=2,'tp'=4] {'ep_0'}, dimensions={0}, use_global_device_ids=true | all-gather | bytes 327680 | tf_op jit(solution)/shard_map/all_gather | solution.py:24
  240.0 2.3 fusion.138
  242.7 1.3 copy-done.3
  243.9 1.6 multiply_convert_fusion
  245.6 3.5 %all_to_all.20 = bf16[32,6,4096]{2,1,0:T(8,128)(2,1)} reshape(bf16[192,4096]{1,0:T(8,128)(2,1)} %reduce-scatter.2.cloned.1.call-done) | data formatting | bytes 3145728 | tf_op jit(solution)/shard_map/all_to_all | solution.py:193
  249.1 10.1 %all-to-all-start.3 = ((bf16[32,6,4096]{2,1,0:T(8,128)(2,1)}), bf16[32,6,4096]{2,1,0:T(8,128)(2,1)S(1)}, u32[]{:S(2)}, u32[]{:S(2)}) async-start(bf16[32,6,4096]{2,1,0:T(8,128)(2,1)} %all_to_all.20), calls=%async_computation.4 | async-start | bytes 4194304 | tf_op jit(solution)/shard_map/all_to_all | solution.py:193
  259.2 36.2 %all-gather.6.cloned.1.call-done = bf16[1024,2048]{0,1:T(8,128)(2,1)} async-done(((bf16[1024,512]{0,1:T(8,128)(2,1)}), bf16[1024,2048]{0,1:T(8,128)(2,1)}) %all-gather.6.cloned.1.call-update) | async-done | bytes 4194320 | tf_op jit(solution)/shard_map/all_gather | solution.py:150
  295.4 9.4 %convolution_convert_fusion.2 = bf16[1024,1024]{1,0:T(8,128)(2,1)} fusion(bf16[1024,2048]{0,1:T(8,128)(2,1)} %all-gather.6.cloned.1.call-done, bf16[2048,1024]{1,0:T(8,128)(2,1)} %param.22), kind=kOutput, calls=%fused_computation.51 | convolution fusion | flops 4296015872 | bytes 10485760 | tf_op jit(solution)/shard_map/dot_general | solution.py:149
  304.8 1.4 all_to_all.22
  306.2 2.0 convolution_multiply_fusion.2
  308.3 1.3 fusion.27
  (132 shorter events, 26.2 us)
Async XLA Ops:
  7.2 150.0 %copy-start = (bf16[1,384,4096]{2,1,0:T(8,128)(2,1)S(1)}, bf16[1,384,4096]{2,1,0:T(8,128)(2,1)}, u32[]{:S(2)}) copy-start(bf16[1,384,4096]{2,1,0:T(8,128)(2,1)} %param.29) | copy-start | bytes 9437188
  69.2 5.4 %copy-start.13 = (u32[128]{0:T(128)S(1)}, u32[128]{0:T(128)}, u32[]{:S(2)}) copy-start(u32[128]{0:T(128)} %constant.100) | copy-start | bytes 1540
  69.2 6.7 %copy-start.10 = (f32[4,1024]{1,0:T(4,128)S(1)}, f32[4,1024]{1,0:T(4,128)}, u32[]{:S(2)}) copy-start(f32[4,1024]{1,0:T(4,128)} %param.21) | copy-start | bytes 49156
  69.2 75.0 %all-to-all-start.2 = ((bf16[4,192,4096]{2,1,0:T(8,128)(2,1)}), bf16[4,192,4096]{2,1,0:T(8,128)(2,1)}, u32[]{:S(2)}, u32[]{:S(2)}) async-start(bf16[4,192,4096]{2,1,0:T(8,128)(2,1)} %stack.3), calls=%async_computation.2 | async-start | bytes 12582912 | tf_op jit(solution)/shard_map/all_to_all | solution.py:181
  74.6 171.0 %reduce-scatter.2.cloned.1.call-start = ((), (), s32[]{:S(2)}) async-start(), calls=%async_computation.6 | async-start | bytes 7864320 | tf_op jit(solution)/shard_map/reduce_scatter | solution.py:187
  104.5 1.4 copy-start.4
  104.5 1.4 copy-start.6
  109.8 2.6 copy-start.8
  109.8 2.6 copy-start.9
  144.3 6.6 %copy-start.12 = (bf16[1,4096,384]{2,1,0:T(8,128)(2,1)S(1)}, bf16[1,4096,384]{2,1,0:T(8,128)(2,1)}, u32[]{:S(2)}) copy-start(bf16[1,4096,384]{2,1,0:T(8,128)(2,1)} %param.28) | copy-start | bytes 9437188
  162.5 133.0 %all-gather.6.cloned.1.call-start = ((), (), s32[]{:S(2)}) async-start(), calls=%async_computation.5 | async-start | bytes 5242880 | tf_op jit(solution)/shard_map/all_gather | solution.py:150
  213.5 26.5 %copy-start.5 = (f32[1024,4,32]{0,2,1:T(8,128)S(1)}, f32[1024,4,32]{0,2,1:T(8,128)}, u32[]{:S(2)}) copy-start(f32[1024,4,32]{0,2,1:T(8,128)} %copy-done.4) | copy-start | bytes 1572868
  213.5 26.5 %copy-start.7 = (f32[1024,4,32]{0,2,1:T(8,128)S(1)}, f32[1024,4,32]{0,2,1:T(8,128)}, u32[]{:S(2)}) copy-start(f32[1024,4,32]{0,2,1:T(8,128)} %copy-done.6) | copy-start | bytes 1572868
  242.3 1.6 copy-start.3
  249.1 10.1 %copy-start.11 = (f32[64,2]{0,1:T(2,128)S(1)}, f32[64,2]{0,1:T(2,128)}, u32[]{:S(2)}) copy-start(f32[64,2]{0,1:T(2,128)} %param.26) | copy-start | bytes 1540
  249.1 55.7 %all-to-all-start.3 = ((bf16[32,6,4096]{2,1,0:T(8,128)(2,1)}), bf16[32,6,4096]{2,1,0:T(8,128)(2,1)S(1)}, u32[]{:S(2)}, u32[]{:S(2)}) async-start(bf16[32,6,4096]{2,1,0:T(8,128)(2,1)} %all_to_all.20), calls=%async_computation.4 | async-start | bytes 4194304 | tf_op jit(solution)/shard_map/all_to_all | solution.py:193
  306.2 2.0 copy-start.2
  306.2 3.3 %copy-start.1 = (bf16[1,384,4096]{2,1,0:T(8,128)(2,1)S(1)}, bf16[1,384,4096]{2,1,0:T(8,128)(2,1)}, u32[]{:S(2)}) copy-start(bf16[1,384,4096]{2,1,0:T(8,128)(2,1)} %param.29) | copy-start | bytes 9437188
Sparse Core Ops, SparseCore 0:
  162.6 62.0 reduce-scatter.1
  245.7 49.7 all-gather.5
